TPU v7x, 32 devices: a whole 2x2x4 slice. The times are simulated.
32 devices in a mesh: ep: 16 (over z, y, x), tp: 2 (over core).
Axes of the slice: x: 2, y: 2, z: 4, core: 2. Of those that a mesh axis runs over, the one named last changes fastest.
Arguments:
- tokens: bfloat16 [4096, 2048], P('ep', 'tp'), may hold values from -6 to 6
- experts: int32 [4096, 16], P('ep'), may hold values from 0 to 65535, as said below
- weights: float32 [4096, 16], P('ep'), may hold values from 0.05 to 1
- up_table: bfloat16 [65536, 2048], P('ep', 'tp'), may hold values from -0.125 to 0.125
- out_table: bfloat16 [65536, 2048], P('ep', 'tp')
- gain: float32 [2048], P('tp'), may hold values from 0.1 to 1.9
Outputs:
- normed: bfloat16 [4096, 2048], P('ep', 'tp')
Inputs may be any that keep to these rules, and one draw needn't show every extreme that they name: An expert number e lies with index e // 4096 of ep. Among the rows of one index of ep, at most 512 chosen experts lie with any one index of ep, and in every draw some index of ep receives exactly 512 from every index.
All inputs are finite; a program needn't handle non-finite values.
Results may differ from a plain program's by a relative error of at most 0.006.
Values may be sent and summed in bfloat16 or wider, within the bound.
A program may use at most 128 MiB of HBM per device.

v0:
```python
import jax
import jax.numpy as jnp
from jax import lax
from jax.sharding import PartitionSpec as P


def owner_ranks(owner, n_ep):
    request_list = owner.shape[0]
    block_len = 512
    block_count = request_list // block_len
    onehot = (owner[:, None] == jnp.arange(n_ep, dtype=jnp.int32)[None, :]).astype(jnp.bfloat16)
    onehot_blocks = onehot.reshape(block_count, block_len, n_ep)
    row_pos = jnp.arange(block_len, dtype=jnp.int32)
    lower = (row_pos[:, None] >= row_pos[None, :]).astype(jnp.bfloat16)
    within = jnp.einsum("ij,bjn->bin", lower, onehot_blocks, preferred_element_type=jnp.float32)
    totals = within[:, block_len - 1, :]
    before = jnp.cumsum(totals, axis=0) - totals
    counted = jnp.sum((within + before[:, None, :]) * onehot_blocks.astype(jnp.float32), axis=2)
    return counted.reshape(request_list).astype(jnp.int32) - 1


def body(tokens, experts, weights, up_table, out_table, gain):
    n_ep = lax.axis_size("ep")
    tok_rows, width = tokens.shape
    slots = experts.shape[1]
    rows_held = up_table.shape[0]
    request_list = tok_rows * slots
    capacity = 2 * request_list // n_ep
    flat = experts.reshape(-1)
    owner = flat // rows_held
    local_row = flat - owner * rows_held
    rank = owner_ranks(owner, n_ep)
    position = owner * capacity + rank
    send_ids = (
        jnp.zeros((n_ep * capacity,), jnp.int32).at[position].set(local_row).reshape(n_ep, capacity)
    )
    source = (
        jnp.full((n_ep * capacity,), -1, jnp.int32)
        .at[position]
        .set(jnp.arange(request_list, dtype=jnp.int32))
    )
    filled = source >= 0
    token_of = jnp.maximum(source, 0) // slots
    picked = jnp.take(tokens, token_of, axis=0)
    send_feat = jnp.where(filled[:, None], picked, jnp.zeros_like(picked)).reshape(
        n_ep, capacity, width
    )
    feat = lax.all_to_all(send_feat, "ep", split_axis=0, concat_axis=0, tiled=True)
    ids = lax.all_to_all(send_ids, "ep", split_axis=0, concat_axis=0, tiled=True)
    partial_value = jnp.einsum(
        "scw,scw->sc", feat, up_table[ids], preferred_element_type=jnp.float32
    )
    dot = lax.psum(partial_value, "tp")
    act = jax.nn.gelu(dot)
    contrib = (act[:, :, None] * out_table[ids]).astype(jnp.bfloat16)
    back = lax.all_to_all(contrib, "ep", split_axis=0, concat_axis=0, tiled=True)
    contrib = jnp.take(back.reshape(n_ep * capacity, width), position, axis=0).reshape(
        tok_rows, slots, width
    )
    mixed = jnp.einsum("tk,tkw->tw", weights, contrib.astype(jnp.float32))
    square = lax.psum(jnp.sum(mixed * mixed, axis=1), "tp")
    scale = lax.rsqrt(square / (width * lax.axis_size("tp")) + 1e-06)
    return (mixed * scale[:, None] * gain[None, :]).astype(jnp.bfloat16)


def solution(mesh):
    placed = (P("ep", "tp"), P("ep", None), P("ep", None), P("ep", "tp"), P("ep", "tp"), P("tp"))
    return jax.shard_map(body, mesh=mesh, in_specs=placed, out_specs=P("ep", "tp"), check_vma=False)
```

profile of v0, /device:TPU:11, one launch (start us, length us, event | category | flops | bytes accessed | tf_op | source)
XLA Modules:
  0.0 936.7 jit_solution(10116794814881835707)
XLA Ops:
  0.0 0.9 copy.15
  0.9 0.1 reshape.212
  1.0 0.1 reshape.213
  1.1 0.1 reshape.214
  1.2 0.3 convolution_bitcast_fusion
  1.5 0.2 fusion.38
  1.7 0.1 multiply_reduce_fusion
  1.8 0.6 convert_add_fusion
  2.5 0.1 compare_select_fusion.1
  2.6 16.1 %scatter_custom_fusion.1 = s32[8192]{0:T(1024)} fusion(s32[4096]{0:T(1024)S(1)} %bitcast.37, s32[4096]{0:T(1024)S(1)} %fusion.28, s32[]{:T(128)} %constant.46.clone.1), kind=kCustom, calls=%fused_computation.72 | custom fusion | bytes 32772 | tf_op jit(solution)/shard_map/scatter | solution.py:35
  18.7 6.6 all-to-all-start.1
  25.4 15.5 %scatter_custom_fusion = s32[8192]{0:T(1024)S(1)} fusion(s32[4096]{0:T(1024)S(1)} %bitcast.38, s32[4096]{0:T(1024)S(1)} %iota.21, s32[]{:T(128)} %constant.74.clone.1), kind=kCustom, calls=%fused_computation.75 | custom fusion | bytes 32772 | tf_op jit(solution)/shard_map/scatter | solution.py:40
  41.1 35.4 %gather_fusion = bf16[8192,1024]{1,0:T(8,128)(2,1)} fusion(bf16[256,1024]{1,0:T(8,128)(2,1)S(1)} %copy-done, s32[8192]{0:T(1024)S(1)} %broadcast_clamp_fusion.1), kind=kCustom, calls=%fused_computation | custom fusion | bytes 33587200 | tf_op jit(solution)/shard_map/jit(_take)/gather | solution.py:44
  76.5 14.5 %select_select_fusion = bf16[16,512,1024]{2,1,0:T(8,128)(2,1)} fusion(bf16[16,512,1024]{2,1,0:T(8,128)(2,1)} %bitcast.34, pred[16,512]{1,0:T(8,128)(4,1)S(1)} %broadcast_in_dim.57, pred[16,512]{1,0:T(8,128)(4,1)S(1)} %broadcast_in_dim.55), kind=kLoop, calls=%fused_computation.10 | loop fusion | flops 16777216 | bytes 33570816 | tf_op jit(solution)/shard_map/jit(_where)/select_n | solution.py:45
  91.0 6.4 all-to-all-start
  97.4 45.0 %gather_fusion.1 = bf16[8192,1024]{1,0:T(8,128)(2,1)} fusion(bf16[4096,1024]{1,0:T(8,128)(2,1)} %param.9, s32[8192]{0:T(1024)S(1)} %broadcast_clamp_fusion), kind=kCustom, calls=%fused_computation.1 | custom fusion | bytes 33587200 | tf_op jit(solution)/shard_map/gather | solution.py:51
  142.5 45.1 %gather_fusion.2 = bf16[8192,1024]{1,0:T(8,128)(2,1)} fusion(bf16[4096,1024]{1,0:T(8,128)(2,1)} %param.10, s32[8192]{0:T(1024)S(1)} %broadcast_clamp_fusion), kind=kCustom, calls=%fused_computation.2 | custom fusion | bytes 33587200 | tf_op jit(solution)/shard_map/gather | solution.py:55
  187.6 288.2 %all-to-all-done = bf16[16,512,1024]{2,1,0:T(8,128)(2,1)} async-done(((bf16[16,512,1024]{2,1,0:T(8,128)(2,1)}), bf16[16,512,1024]{2,1,0:T(8,128)(2,1)}, u32[]{:S(2)}, u32[]{:S(2)}) %all-to-all-start) | async-done | bytes 16777248 | tf_op jit(solution)/shard_map/all_to_all | solution.py:48
  475.8 13.2 %fusion.1 = f32[16,512]{1,0:T(8,128)S(1)} fusion(bf16[16,512,1024]{2,1,0:T(8,128)(2,1)} %all-to-all-done, bf16[16,512,1024]{2,1,0:T(8,128)(2,1)} %bitcast.33), kind=kLoop, calls=%fused_computation.9 | loop fusion | flops 33546240 | bytes 33587200 | tf_op jit(solution)/shard_map/scw,scw->sc/dot_general | solution.py:50
  489.0 5.6 psum.14
  494.6 14.7 %fusion = bf16[16,512,1024]{2,1,0:T(8,128)(2,1)} fusion(bf16[16,512,1024]{2,1,0:T(8,128)(2,1)} %bitcast.32, f32[16,512]{1,0:T(8,128)S(1)} %fusion.20), kind=kLoop, calls=%fused_computation.7 | loop fusion | flops 25165824 | bytes 33587200 | tf_op jit(solution)/shard_map/convert_element_type | solution.py:55
  509.3 7.5 all-to-all-start.2
  516.8 0.1 sub.37
  516.9 0.1 copy.16
  517.0 0.1 copy.17
  517.2 0.1 copy.24
  517.4 381.4 %all-to-all-done.2 = bf16[16,512,1024]{2,1,0:T(8,128)(2,1)} async-done(((bf16[16,512,1024]{2,1,0:T(8,128)(2,1)}), bf16[16,512,1024]{2,1,0:T(8,128)(2,1)}, u32[]{:S(2)}, u32[]{:S(2)}) %all-to-all-start.2) | async-done | bytes 16777248 | tf_op jit(solution)/shard_map/all_to_all | solution.py:56
  898.8 28.9 %gather_fusion.3 = bf16[4096,1024]{1,0:T(8,128)(2,1)} fusion(bf16[8192,1024]{1,0:T(8,128)(2,1)} %bitcast.9, s32[4096]{0:T(1024)S(1)} %broadcast_clamp_fusion.2), kind=kCustom, calls=%fused_computation.3 | custom fusion | bytes 16793600 | tf_op jit(solution)/shard_map/jit(_take)/gather | solution.py:57
  927.6 4.3 fusion.2
  932.0 0.2 fusion.6
  932.2 3.4 psum.15
  935.6 1.1 fusion.8
  (31 shorter events, 0.3 us)
Async XLA Ops:
  0.0 41.1 %copy-start = (bf16[256,1024]{1,0:T(8,128)(2,1)S(1)}, bf16[256,1024]{1,0:T(8,128)(2,1)}, u32[]{:S(2)}) copy-start(bf16[256,1024]{1,0:T(8,128)(2,1)} %param.6) | copy-start | bytes 1572868
  2.6 38.3 %copy-start.4 = (s32[4096,1]{0,1:T(1,128)}, s32[4096,1]{0,1:T(1,128)S(1)}, u32[]{:S(2)}) copy-start(s32[4096,1]{0,1:T(1,128)S(1)} %compare_select_fusion.1) | copy-start | bytes 49156
  18.7 72.3 %all-to-all-start.1 = ((s32[16,1,512]{2,1,0:T(1,128)}), s32[16,1,512]{2,1,0:T(1,128)S(1)}, u32[]{:S(2)}, u32[]{:S(2)}) async-start(s32[16,1,512]{2,1,0:T(1,128)} %bitcast.4), calls=%async_computation.1 | async-start | bytes 65536 | tf_op jit(solution)/shard_map/all_to_all | solution.py:49
  91.0 384.7 %all-to-all-start = ((bf16[16,512,1024]{2,1,0:T(8,128)(2,1)}), bf16[16,512,1024]{2,1,0:T(8,128)(2,1)}, u32[]{:S(2)}, u32[]{:S(2)}) async-start(bf16[16,512,1024]{2,1,0:T(8,128)(2,1)} %select_select_fusion), calls=%async_computation | async-start | bytes 33554432 | tf_op jit(solution)/shard_map/all_to_all | solution.py:48
  509.3 7.5 copy-start.2
  509.3 7.7 copy-start.3
  509.3 7.9 copy-start.6
  509.3 8.0 copy-start.5
  509.3 389.4 %all-to-all-start.2 = ((bf16[16,512,1024]{2,1,0:T(8,128)(2,1)}), bf16[16,512,1024]{2,1,0:T(8,128)(2,1)}, u32[]{:S(2)}, u32[]{:S(2)}) async-start(bf16[16,512,1024]{2,1,0:T(8,128)(2,1)} %fusion), calls=%async_computation.2 | async-start | bytes 33554432 | tf_op jit(solution)/shard_map/all_to_all | solution.py:56
  898.8 37.9 %copy-start.1 = (bf16[256,1024]{1,0:T(8,128)(2,1)S(1)}, bf16[256,1024]{1,0:T(8,128)(2,1)}, u32[]{:S(2)}) copy-start(bf16[256,1024]{1,0:T(8,128)(2,1)} %param.6) | copy-start | bytes 1572868
  927.6 8.0 copy-start.7
where the time goes:
time: 939 us; the launch traced here: 937 us
  waiting for transfers between devices  670 us (71%)
  local copies, waits for them, and re-layouts  188 us (20%)
  other arithmetic  44.9 us (5%)
  starting transfers between devices  20.5 us (2%)
    all_to_all x1, waiting for transfers between devices, body(): lax.all_to_all(contrib, 'ep', split_axis=0, concat_axis=0, tiled=True)  381 us
    all_to_all x1, waiting for transfers between devices, body(): lax.all_to_all(send_feat, 'ep', split_axis=0, concat_axis=0, tiled=True)  288 us
    gather x1, local copies, waits for them, and re-layouts, body(): contrib = (act[:, :, None] * out_table[ids]).astype(jnp.bfloat16)  45.1 us
    gather x1, local copies, waits for them, and re-layouts, body(): up_table[ids]  45 us
    gather x1, local copies, waits for them, and re-layouts, body(): picked = jnp.take(tokens, token_of, axis=0)  35.4 us
    gather x1, local copies, waits for them, and re-layouts, body(): jnp.take(back.reshape(n_ep * capacity, width), position, axis=0)  28.9 us
  transfers between devices with their start and end apart: 3, of which 2 were waited for; matrix products, arithmetic and copies ran while one was open for 17% of the time, Pallas kernels for 0%

commit v1 on v0

v1 whole, which is shorter than its diff:
```python
import functools

import jax
import jax.numpy as jnp
from jax import lax
from jax.experimental import pallas as pl
from jax.experimental.pallas import tpu as pltpu
from jax.sharding import PartitionSpec as P

LANES = 128


def owner_ranks(owner, n_ep):
    request_list = owner.shape[0]
    block_len = 512
    block_count = request_list // block_len
    onehot = (owner[:, None] == jnp.arange(n_ep, dtype=jnp.int32)[None, :]).astype(jnp.bfloat16)
    onehot_blocks = onehot.reshape(block_count, block_len, n_ep)
    row_pos = jnp.arange(block_len, dtype=jnp.int32)
    lower = (row_pos[:, None] >= row_pos[None, :]).astype(jnp.bfloat16)
    within = jnp.einsum("ij,bjn->bin", lower, onehot_blocks, preferred_element_type=jnp.float32)
    totals = within[:, block_len - 1, :]
    before = jnp.cumsum(totals, axis=0) - totals
    counted = jnp.sum((within + before[:, None, :]) * onehot_blocks.astype(jnp.float32), axis=2)
    return counted.reshape(request_list).astype(jnp.int32) - 1


def dots_kernel(rows_held, capacity, list_ref, tok_ref, up_ref, dot_ref, prod):
    sub = tok_ref.shape[1]
    base = pl.program_id(0) * capacity
    unroll = 16
    for block in range(capacity // LANES):

        def some(g, carry):
            for u in range(unroll):
                k = g * unroll + u
                word = list_ref[base + block * LANES + k]
                a = tok_ref[word // rows_held].astype(jnp.float32)
                b = up_ref[word % rows_held].astype(jnp.float32)
                prod[pl.ds(pl.multiple_of(k * sub, sub), sub), :] = a * b
            return carry

        lax.fori_loop(0, LANES // unroll, some, 0)
        if sub == 1:
            total = prod[...]
        else:
            total = prod[pl.ds(0, LANES, stride=sub), :]
            for s in range(1, sub):
                total = total + prod[pl.ds(s, LANES, stride=sub), :]
        dot_ref[0, pl.ds(block, 1), :] = jnp.sum(total.T, axis=0, keepdims=True)


def request_dots(words, tok_all, up, capacity, n_ep):
    rows_held, sub, _ = up.shape
    tok_rows = tok_all.shape[0] // n_ep
    return pl.pallas_call(
        functools.partial(dots_kernel, rows_held, capacity),
        grid_spec=pltpu.PrefetchScalarGridSpec(
            num_scalar_prefetch=1,
            grid=(n_ep,),
            in_specs=[
                pl.BlockSpec((tok_rows, sub, LANES), lambda i, w: (i, 0, 0)),
                pl.BlockSpec((rows_held, sub, LANES), lambda i, w: (0, 0, 0)),
            ],
            out_specs=pl.BlockSpec((1, capacity // LANES, LANES), lambda i, w: (i, 0, 0)),
            scratch_shapes=[pltpu.VMEM((LANES * sub, LANES), jnp.float32)],
        ),
        out_shape=jax.ShapeDtypeStruct((n_ep, capacity // LANES, LANES), jnp.float32),
        name="request_dots",
    )(words, tok_all, up)


def mix_kernel(rows_held, capacity, group, tok_rows, list_ref, coef_ref, table_ref, mix_ref, acc):
    first = pl.program_id(0) * group

    def clear(i, carry):
        acc[pl.ds(i * LANES, LANES)] = jnp.zeros((LANES,) + acc.shape[1:], acc.dtype)
        return carry

    lax.fori_loop(0, acc.shape[0] // LANES, clear, 0)

    def step(j, carry):
        places, sums = [], []
        for s in range(group):
            at = (first + s) * capacity + j
            word = list_ref[at]
            place = s * tok_rows + word // rows_held
            row = table_ref[word % rows_held].astype(jnp.float32)
            places.append(place)
            sums.append(acc[place] + coef_ref[at] * row)
        for place, total in zip(places, sums):
            acc[place] = total
        return carry

    lax.fori_loop(0, capacity, step, 0)

    def emit(i, carry):
        mix_ref[pl.ds(i * LANES, LANES)] = acc[pl.ds(i * LANES, LANES)].astype(mix_ref.dtype)
        return carry

    lax.fori_loop(0, acc.shape[0] // LANES, emit, 0)


def mix_rows(words, coef, table, capacity, n_ep, tok_rows):
    rows_held, sub, _ = table.shape
    group = 16
    return pl.pallas_call(
        functools.partial(mix_kernel, rows_held, capacity, group, tok_rows),
        grid_spec=pltpu.PrefetchScalarGridSpec(
            num_scalar_prefetch=2,
            grid=(n_ep // group,),
            in_specs=[pl.BlockSpec((rows_held, sub, LANES), lambda i, w, c: (0, 0, 0))],
            out_specs=pl.BlockSpec((group * tok_rows, sub, LANES), lambda i, w, c: (i, 0, 0)),
            scratch_shapes=[pltpu.VMEM((group * tok_rows, sub, LANES), jnp.float32)],
        ),
        out_shape=jax.ShapeDtypeStruct((n_ep * tok_rows, sub, LANES), jnp.bfloat16),
        name="mix_rows",
    )(words, coef, table)


def body(tokens, experts, weights, up_table, out_table, gain):
    n_ep = lax.axis_size("ep")
    tok_rows, width = tokens.shape
    slots = experts.shape[1]
    rows_held = up_table.shape[0]
    sub = width // LANES
    request_list = tok_rows * slots
    capacity = 2 * request_list // n_ep
    tok_all = lax.all_gather(tokens.reshape(tok_rows, sub, LANES), "ep", axis=0, tiled=True)
    flat = experts.reshape(-1)
    owner = flat // rows_held
    local_row = flat - owner * rows_held
    position = owner * capacity + owner_ranks(owner, n_ep)
    token_of = jnp.arange(request_list, dtype=jnp.int32) // slots
    send_words = (
        jnp.zeros((n_ep * capacity,), jnp.int32)
        .at[position]
        .set(token_of * rows_held + local_row, unique_indices=True)
    )
    send_weights = (
        jnp.zeros((n_ep * capacity,), jnp.float32)
        .at[position]
        .set(weights.reshape(-1), unique_indices=True)
    )
    words = lax.all_to_all(send_words.reshape(n_ep, capacity), "ep", 0, 0, tiled=True).reshape(-1)
    scales = lax.all_to_all(send_weights.reshape(n_ep, capacity), "ep", 0, 0, tiled=True)
    up = up_table.reshape(rows_held, sub, LANES)
    out = out_table.reshape(rows_held, sub, LANES)
    partial_value = request_dots(words, tok_all, up, capacity, n_ep)
    dot = lax.psum(partial_value, "tp")
    coef = (scales.reshape(dot.shape) * jax.nn.gelu(dot)).reshape(-1)
    part = mix_rows(words, coef, out, capacity, n_ep, tok_rows)
    mixed = lax.psum_scatter(part, "ep", scatter_dimension=0, tiled=True).astype(jnp.float32)
    square = lax.psum(jnp.sum(mixed * mixed, axis=(1, 2)), "tp")
    scale = lax.rsqrt(square / (width * lax.axis_size("tp")) + 1e-06)
    normed = mixed * scale[:, None, None] * gain.reshape(1, sub, LANES)
    return normed.astype(jnp.bfloat16).reshape(tok_rows, width)


def solution(mesh):
    placed = (P("ep", "tp"), P("ep", None), P("ep", None), P("ep", "tp"), P("ep", "tp"), P("tp"))
    return jax.shard_map(body, mesh=mesh, in_specs=placed, out_specs=P("ep", "tp"), check_vma=False)
```

time: 939 us -> 477 us (0.51)
  waiting for transfers between devices: 670 us -> 226 us
  Pallas kernels: 0 us -> 154 us
  local copies, waits for them, and re-layouts: 188 us -> 55.3 us
  other arithmetic: 44.9 us -> 4.55 us
  between operations: 0.23 us -> 13.5 us
    all_to_all x3 -> x2, waiting for transfers between devices: 670 us -> 0.01 us  [the longest x1 0.01 us: body(): lax.all_to_all(send_words.reshape(n_ep, capacity), 'ep', 0, 0, tiled=True)]
    reduce_scatter x0 -> x1, waiting for transfers between devices: none -> 180 us  [body(): lax.psum_scatter(part, 'ep', scatter_dimension=0, tiled=True)]
    gather x4 -> x0, local copies, waits for them, and re-layouts: 154 us -> none  [the longest x1 45.1 us: body(): contrib = (act[:, :, None] * out_table[ids]).astype(jnp.bfloat16)]
    pallas_call x0 -> x2, Pallas kernels: none -> 154 us  [the longest x1 79.4 us: mix_rows(): pl.pallas_call(functools.partial(mix_kernel, rows_held, capacity, group,...]
    all_gather x0 -> x1, waiting for transfers between devices: none -> 46.3 us  [body(): lax.all_gather(tokens.reshape(tok_rows, sub, LANES), 'ep', axis=0, tiled=...]
    unnamed x19 -> x11, local copies, waits for them, and re-layouts: 1.07 us -> 22.6 us
    select_n x3 -> x1, other arithmetic: 14.6 us -> 0.1 us  [body(): send_words = jnp.zeros((n_ep * capacity,), jnp.int32).at[position].set(to...]
    convert_element_type x2 -> x1, other arithmetic: 15.7 us -> 1.38 us  [body(): return normed.astype(jnp.bfloat16).reshape(tok_rows, width)]
  transfers between devices with their start and end apart: 3 -> 4, of which waited for: 2 -> 2; matrix products, arithmetic and copies ran while one was open for 17% -> 11% of each run, Pallas kernels for 0% -> 16%
where the time goes in v1:
time: 477 us; the launch traced here: 476 us
  waiting for transfers between devices  226 us (47%)
  Pallas kernels  154 us (32%)
  local copies, waits for them, and re-layouts  55.3 us (12%)
  between operations  13.5 us (3%)
  starting transfers between devices  13 us (3%)
  blocking collectives  9.5 us (2%)
    reduce_scatter x1, waiting for transfers between devices, body(): lax.psum_scatter(part, 'ep', scatter_dimension=0, tiled=True)  180 us
    pallas_call x1, Pallas kernels, mix_rows(): pl.pallas_call(functools.partial(mix_kernel, rows_held, capacity, group,...  79.4 us
    pallas_call x1, Pallas kernels, request_dots(): pl.pallas_call(functools.partial(dots_kernel, rows_held, capacity), grid_...  74.8 us
    all_gather x1, waiting for transfers between devices, body(): lax.all_gather(tokens.reshape(tok_rows, sub, LANES), 'ep', axis=0, tiled=...  46.3 us
    unnamed x11, local copies, waits for them, and re-layouts  22.6 us
    scatter x1, local copies, waits for them, and re-layouts, body(): send_weights = jnp.zeros((n_ep * capacity,), jnp.float32).at[position].se...  16.1 us
    scatter x1, local copies, waits for them, and re-layouts, body(): send_words = jnp.zeros((n_ep * capacity,), jnp.int32).at[position].set(to...  16.1 us
  transfers between devices with their start and end apart: 4, of which 2 were waited for; matrix products, arithmetic and copies ran while one was open for 11% of the time, Pallas kernels for 16%

profile of v1, /device:TPU:11, one launch (start us, length us, event | category | flops | bytes accessed | tf_op | source)
XLA Modules:
  0.0 476.3 jit_solution(6898948228269882852)
XLA Ops:
  6.5 1.9 copy.16
  8.5 0.0 all-gather.2.cloned.1.call-update
  8.5 0.8 copy.11
  9.3 0.1 reshape.177
  9.4 0.1 reshape.176
  9.5 0.1 reshape.175
  9.7 0.3 convolution_bitcast_fusion
  10.0 0.2 fusion.31
  10.2 0.1 multiply_reduce_fusion
  10.4 0.1 compare_select_fusion
  10.5 16.1 %scatter_custom_fusion = s32[8192]{0:T(1024)} fusion(s32[4096]{0:T(1024)S(1)} %bitcast.41, s32[4096]{0:T(1024)S(1)} %fusion.18, s32[]{:T(128)} %constant.41.clone.1), kind=kCustom, calls=%fused_computation.56 | custom fusion | bytes 32772 | tf_op jit(solution)/shard_map/scatter | solution.py:138
  26.5 6.6 %all-to-all-start = ((s32[16,1,512]{2,1,0:T(1,128)}), s32[16,1,512]{2,1,0:T(1,128)S(1)}, u32[]{:S(2)}, u32[]{:S(2)}) async-start(s32[16,1,512]{2,1,0:T(1,128)} %bitcast.3), calls=%async_computation | async-start | bytes 65536 | tf_op jit(solution)/shard_map/all_to_all | solution.py:145
  33.2 0.8 copy.14
  34.0 0.1 reshape.198
  34.1 16.1 %scatter_custom_fusion.1 = f32[8192]{0:T(1024)} fusion(s32[4096]{0:T(1024)S(1)} %bitcast.42, f32[4096]{0:T(1024)S(1)} %reshape.198, f32[]{:T(128)} %constant.47.clone.1), kind=kCustom, calls=%fused_computation.51 | custom fusion | bytes 32772 | tf_op jit(solution)/shard_map/scatter | solution.py:143
  50.2 0.0 all-to-all-done
  50.2 6.4 %all-to-all-start.1 = ((f32[16,1,512]{2,1,0:T(1,128)}), f32[16,1,512]{2,1,0:T(1,128)S(1)}, u32[]{:S(2)}, u32[]{:S(2)}) async-start(f32[16,1,512]{2,1,0:T(1,128)} %bitcast.5), calls=%async_computation.1 | async-start | bytes 65536 | tf_op jit(solution)/shard_map/all_to_all | solution.py:146
  56.6 0.0 reduce-scatter.2.cloned.1.call-start
  56.6 8.9 %copy.17 = bf16[512,8,8,128]{3,2,1,0:T(8,128)(2,1)} copy(bf16[512,8,8,128]{3,1,2,0:T(8,128)(2,1)} %bitcast.31) | data formatting | bytes 16777216
  65.5 9.3 %copy.18 = bf16[512,8,8,128]{3,2,1,0:T(8,128)(2,1)} copy(bf16[512,8,8,128]{3,1,2,0:T(8,128)(2,1)} %bitcast.32) | data formatting | bytes 16777216
  74.8 46.3 %all-gather.2.cloned.1.call-done.tok_ref = bf16[4096,8,128]{2,1,0:T(8,128)(2,1)} async-done(((bf16[256,8,128]{2,1,0:T(8,128)(2,1)}), bf16[4096,8,128]{2,1,0:T(8,128)(2,1)}) %all-gather.2.cloned.1.call-update) | async-done | bytes 8388624 | tf_op jit(solution)/shard_map/all_gather | solution.py:129
  121.1 74.8 %request_dots.1 = f32[16,4,128]{2,1,0:T(4,128)} custom-call(s32[8192]{0:T(1024)} %bitcast.36, bf16[4096,8,128]{2,1,0:T(8,128)(2,1)} %all-gather.2.cloned.1.call-done.tok_ref, bf16[4096,8,128]{2,1,0:T(8,128)(2,1)} %bitcast.30), custom_call_target="tpu_custom_call" | custom-call | tf_op jit(solution)/shard_map/request_dots/pallas_call | solution.py:56
  195.8 6.5 %psum.14 = f32[16,4,128]{2,1,0:T(4,128)S(1)} all-reduce(f32[16,4,128]{2,1,0:T(4,128)} %request_dots.1), channel_id=1, replica_groups=mesh['ep'=16,'tp'=2] {'tp'}, use_global_device_ids=true, to_apply=%region_4.5 | all-reduce | flops 8192 | bytes 65536 | tf_op jit(solution)/shard_map/psum | solution.py:150
  202.3 0.0 all-to-all-done.1
  202.3 0.6 fusion.15
  202.9 79.4 %mix_rows.1 = bf16[4096,8,128]{2,1,0:T(8,128)(2,1)} custom-call(s32[8192]{0:T(1024)} %bitcast.37, f32[8192]{0:T(1024)} %bitcast.38, bf16[4096,8,128]{2,1,0:T(8,128)(2,1)} %bitcast.29), custom_call_target="tpu_custom_call" | custom-call | tf_op jit(solution)/shard_map/mix_rows/pallas_call | solution.py:107
  282.4 0.0 reduce-scatter.2.cloned.1.call-update
  282.4 179.7 %reduce-scatter.2.cloned.1.call-done = bf16[256,8,128]{2,1,0:T(8,128)(2,1)} async-done(((bf16[4096,8,128]{2,1,0:T(8,128)(2,1)}), bf16[256,8,128]{2,1,0:T(8,128)(2,1)}) %reduce-scatter.2.cloned.1.call-update) | async-done | bytes 524304 | tf_op jit(solution)/shard_map/reduce_scatter | solution.py:153
  462.1 2.1 fusion
  464.2 3.0 psum.15
  467.2 1.4 fusion.2
  468.6 0.9 copy.21
  (10 shorter events, 0.1 us)
Async XLA Ops:
  6.5 114.5 %all-gather.2.cloned.1.call-start = ((), (), s32[]{:S(2)}) async-start(), calls=%async_computation.3 | async-start | bytes 8912896 | tf_op jit(solution)/shard_map/all_gather | solution.py:129
  26.5 23.7 %all-to-all-start = ((s32[16,1,512]{2,1,0:T(1,128)}), s32[16,1,512]{2,1,0:T(1,128)S(1)}, u32[]{:S(2)}, u32[]{:S(2)}) async-start(s32[16,1,512]{2,1,0:T(1,128)} %bitcast.3), calls=%async_computation | async-start | bytes 65536 | tf_op jit(solution)/shard_map/all_to_all | solution.py:145
  50.2 15.3 %copy-start = (s32[16,1,512]{2,1,0:T(1,128)}, s32[16,1,512]{2,1,0:T(1,128)S(1)}, u32[]{:S(2)}) copy-start(s32[16,1,512]{2,1,0:T(1,128)S(1)} %all-to-all-done) | copy-start | bytes 98308
  50.2 152.1 %all-to-all-start.1 = ((f32[16,1,512]{2,1,0:T(1,128)}), f32[16,1,512]{2,1,0:T(1,128)S(1)}, u32[]{:S(2)}, u32[]{:S(2)}) async-start(f32[16,1,512]{2,1,0:T(1,128)} %bitcast.5), calls=%async_computation.1 | async-start | bytes 65536 | tf_op jit(solution)/shard_map/all_to_all | solution.py:146
  56.6 405.5 %reduce-scatter.2.cloned.1.call-start = ((), (), s32[]{:S(2)}) async-start(), calls=%async_computation.4 | async-start | bytes 8912896 | tf_op jit(solution)/shard_map/reduce_scatter | solution.py:153
  282.4 184.9 %copy-start.1 = (f32[1024]{0:T(1024)S(1)}, f32[1024]{0:T(1024)}, u32[]{:S(2)}) copy-start(f32[1024]{0:T(1024)} %param.11) | copy-start | bytes 12292
Sparse Core Ops, SparseCore 0:
  10.1 110.9 all-gather.1
  282.5 179.5 reduce-scatter.1

commit v2 on v1

--- a/solution.py
+++ b/solution.py
@@ -1,4 +1,5 @@
 import functools
+import math
 
 import jax
 import jax.numpy as jnp
@@ -25,18 +26,18 @@
     return counted.reshape(request_list).astype(jnp.int32) - 1
 
 
-def dots_kernel(rows_held, capacity, list_ref, tok_ref, up_ref, dot_ref, prod):
+def dots_kernel(capacity, place_ref, row_ref, tok_ref, up_ref, dot_ref, prod):
     sub = tok_ref.shape[1]
     base = pl.program_id(0) * capacity
-    unroll = 16
+    unroll = 32
     for block in range(capacity // LANES):
 
         def some(g, carry):
             for u in range(unroll):
                 k = g * unroll + u
-                word = list_ref[base + block * LANES + k]
-                a = tok_ref[word // rows_held].astype(jnp.float32)
-                b = up_ref[word % rows_held].astype(jnp.float32)
+                at = base + block * LANES + k
+                a = tok_ref[place_ref[at]].astype(jnp.float32)
+                b = up_ref[row_ref[at]].astype(jnp.float32)
                 prod[pl.ds(pl.multiple_of(k * sub, sub), sub), :] = a * b
             return carry
 
@@ -50,27 +51,27 @@
         dot_ref[0, pl.ds(block, 1), :] = jnp.sum(total.T, axis=0, keepdims=True)
 
 
-def request_dots(words, tok_all, up, capacity, n_ep):
+def request_dots(places, rows, tok_all, up, capacity, n_ep):
     rows_held, sub, _ = up.shape
     tok_rows = tok_all.shape[0] // n_ep
     return pl.pallas_call(
-        functools.partial(dots_kernel, rows_held, capacity),
+        functools.partial(dots_kernel, capacity),
         grid_spec=pltpu.PrefetchScalarGridSpec(
-            num_scalar_prefetch=1,
+            num_scalar_prefetch=2,
             grid=(n_ep,),
             in_specs=[
-                pl.BlockSpec((tok_rows, sub, LANES), lambda i, w: (i, 0, 0)),
-                pl.BlockSpec((rows_held, sub, LANES), lambda i, w: (0, 0, 0)),
+                pl.BlockSpec((tok_rows, sub, LANES), lambda i, p, r: (i, 0, 0)),
+                pl.BlockSpec((rows_held, sub, LANES), lambda i, p, r: (0, 0, 0)),
             ],
-            out_specs=pl.BlockSpec((1, capacity // LANES, LANES), lambda i, w: (i, 0, 0)),
+            out_specs=pl.BlockSpec((1, capacity // LANES, LANES), lambda i, p, r: (i, 0, 0)),
             scratch_shapes=[pltpu.VMEM((LANES * sub, LANES), jnp.float32)],
         ),
         out_shape=jax.ShapeDtypeStruct((n_ep, capacity // LANES, LANES), jnp.float32),
         name="request_dots",
-    )(words, tok_all, up)
+    )(places, rows, tok_all, up)
 
 
-def mix_kernel(rows_held, capacity, group, tok_rows, list_ref, coef_ref, table_ref, mix_ref, acc):
+def mix_kernel(capacity, group, place_ref, row_ref, coef_ref, table_ref, mix_ref, acc):
     first = pl.program_id(0) * group
 
     def clear(i, carry):
@@ -83,9 +84,8 @@
         places, sums = [], []
         for s in range(group):
             at = (first + s) * capacity + j
-            word = list_ref[at]
-            place = s * tok_rows + word // rows_held
-            row = table_ref[word % rows_held].astype(jnp.float32)
+            place = place_ref[at]
+            row = table_ref[row_ref[at]].astype(jnp.float32)
             places.append(place)
             sums.append(acc[place] + coef_ref[at] * row)
         for place, total in zip(places, sums):
@@ -101,21 +101,20 @@
     lax.fori_loop(0, acc.shape[0] // LANES, emit, 0)
 
 
-def mix_rows(words, coef, table, capacity, n_ep, tok_rows):
+def mix_rows(places, rows, coef, table, capacity, n_ep, tok_rows, group):
     rows_held, sub, _ = table.shape
-    group = 16
     return pl.pallas_call(
-        functools.partial(mix_kernel, rows_held, capacity, group, tok_rows),
+        functools.partial(mix_kernel, capacity, group),
         grid_spec=pltpu.PrefetchScalarGridSpec(
-            num_scalar_prefetch=2,
+            num_scalar_prefetch=3,
             grid=(n_ep // group,),
-            in_specs=[pl.BlockSpec((rows_held, sub, LANES), lambda i, w, c: (0, 0, 0))],
-            out_specs=pl.BlockSpec((group * tok_rows, sub, LANES), lambda i, w, c: (i, 0, 0)),
+            in_specs=[pl.BlockSpec((rows_held, sub, LANES), lambda i, p, r, c: (0, 0, 0))],
+            out_specs=pl.BlockSpec((group * tok_rows, sub, LANES), lambda i, p, r, c: (i, 0, 0)),
             scratch_shapes=[pltpu.VMEM((group * tok_rows, sub, LANES), jnp.float32)],
         ),
         out_shape=jax.ShapeDtypeStruct((n_ep * tok_rows, sub, LANES), jnp.bfloat16),
         name="mix_rows",
-    )(words, coef, table)
+    )(places, rows, coef, table)
 
 
 def body(tokens, experts, weights, up_table, out_table, gain):
@@ -142,14 +141,19 @@
         .at[position]
         .set(weights.reshape(-1), unique_indices=True)
     )
-    words = lax.all_to_all(send_words.reshape(n_ep, capacity), "ep", 0, 0, tiled=True).reshape(-1)
+    words = lax.all_to_all(send_words.reshape(n_ep, capacity), "ep", 0, 0, tiled=True)
+    token_at = words // rows_held
+    row_at = (words % rows_held).reshape(-1)
+    group = math.gcd(n_ep, 16)
+    first = (jnp.arange(n_ep, dtype=jnp.int32) % group) * tok_rows
+    place_at = (token_at + first[:, None]).reshape(-1)
     scales = lax.all_to_all(send_weights.reshape(n_ep, capacity), "ep", 0, 0, tiled=True)
     up = up_table.reshape(rows_held, sub, LANES)
     out = out_table.reshape(rows_held, sub, LANES)
-    partial_value = request_dots(words, tok_all, up, capacity, n_ep)
+    partial_value = request_dots(token_at.reshape(-1), row_at, tok_all, up, capacity, n_ep)
     dot = lax.psum(partial_value, "tp")
     coef = (scales.reshape(dot.shape) * jax.nn.gelu(dot)).reshape(-1)
-    part = mix_rows(words, coef, out, capacity, n_ep, tok_rows)
+    part = mix_rows(place_at, row_at, coef, out, capacity, n_ep, tok_rows, group)
     mixed = lax.psum_scatter(part, "ep", scatter_dimension=0, tiled=True).astype(jnp.float32)
     square = lax.psum(jnp.sum(mixed * mixed, axis=(1, 2)), "tp")
     scale = lax.rsqrt(square / (width * lax.axis_size("tp")) + 1e-06)

time: 477 us -> 400 us (0.84)
  Pallas kernels: 154 us -> 76.6 us
    pallas_call x2, Pallas kernels: 154 us -> 76.6 us  [the longest x1 41.3 us: mix_rows(): pl.pallas_call(functools.partial(mix_kernel, capacity, group), grid_spec=...]
  transfers between devices with their start and end apart: 4 -> 4, of which waited for: 2 -> 2; matrix products, arithmetic and copies ran while one was open for 11% -> 13% of each run, Pallas kernels for 16% -> 9%
where the time goes in v2:
time: 400 us; the launch traced here: 399 us
  waiting for transfers between devices  226 us (56%)
  Pallas kernels  76.6 us (19%)
  local copies, waits for them, and re-layouts  54.7 us (14%)
  between operations  13.5 us (3%)
  starting transfers between devices  13 us (3%)
  blocking collectives  9.51 us (2%)
  other arithmetic  5.23 us (1%)
    reduce_scatter x1, waiting for transfers between devices, body(): lax.psum_scatter(part, 'ep', scatter_dimension=0, tiled=True)  180 us
    all_gather x1, waiting for transfers between devices, body(): lax.all_gather(tokens.reshape(tok_rows, sub, LANES), 'ep', axis=0, tiled=...  45.9 us
    pallas_call x1, Pallas kernels, mix_rows(): pl.pallas_call(functools.partial(mix_kernel, capacity, group), grid_spec=...  41.3 us
    pallas_call x1, Pallas kernels, request_dots(): pl.pallas_call(functools.partial(dots_kernel, capacity), grid_spec=pltpu....  35.3 us
    unnamed x11, local copies, waits for them, and re-layouts  22.2 us
    scatter x1, local copies, waits for them, and re-layouts, body(): send_words = jnp.zeros((n_ep * capacity,), jnp.int32).at[position].set(to...  16.1 us
    scatter x1, local copies, waits for them, and re-layouts, body(): send_weights = jnp.zeros((n_ep * capacity,), jnp.float32).at[position].se...  16.1 us
  transfers between devices with their start and end apart: 4, of which 2 were waited for; matrix products, arithmetic and copies ran while one was open for 13% of the time, Pallas kernels for 9%

profile of v2, /device:TPU:11, one launch (start us, length us, event | category | flops | bytes accessed | tf_op | source)
XLA Modules:
  0.0 398.6 jit_solution(16698907273081976393)
XLA Ops:
  6.5 1.9 copy.17
  8.5 0.0 all-gather.2.cloned.1.call-update
  8.5 0.8 copy.11
  9.3 0.1 reshape.190
  9.4 0.1 reshape.189
  9.5 0.1 reshape.188
  9.7 0.3 convolution_bitcast_fusion
  10.0 0.2 fusion.35
  10.2 0.1 multiply_reduce_fusion
  10.4 0.1 compare_select_fusion
  10.5 16.1 %scatter_custom_fusion = s32[8192]{0:T(1024)} fusion(s32[4096]{0:T(1024)S(1)} %bitcast.44, s32[4096]{0:T(1024)S(1)} %fusion.20, s32[]{:T(128)} %constant.74.clone.1), kind=kCustom, calls=%fused_computation.65 | custom fusion | bytes 32772 | tf_op jit(solution)/shard_map/scatter | solution.py:137
  26.5 6.6 %all-to-all-start = ((s32[16,1,512]{2,1,0:T(1,128)}), s32[16,1,512]{2,1,0:T(1,128)S(1)}, u32[]{:S(2)}, u32[]{:S(2)}) async-start(s32[16,1,512]{2,1,0:T(1,128)} %bitcast.3), calls=%async_computation | async-start | bytes 65536 | tf_op jit(solution)/shard_map/all_to_all | solution.py:144
  33.2 0.1 broadcast_bitcast_fusion
  33.3 0.8 copy.14
  34.1 0.1 reshape.210
  34.2 8.8 %copy.18 = bf16[512,8,8,128]{3,2,1,0:T(8,128)(2,1)} copy(bf16[512,8,8,128]{3,1,2,0:T(8,128)(2,1)} %bitcast.34) | data formatting | bytes 16777216
  43.0 8.8 %copy.19 = bf16[512,8,8,128]{3,2,1,0:T(8,128)(2,1)} copy(bf16[512,8,8,128]{3,1,2,0:T(8,128)(2,1)} %bitcast.35) | data formatting | bytes 16777216
  51.8 16.1 %scatter_custom_fusion.1 = f32[8192]{0:T(1024)} fusion(s32[4096]{0:T(1024)S(1)} %bitcast.45, f32[4096]{0:T(1024)S(1)} %reshape.210, f32[]{:T(128)} %constant.80.clone.1), kind=kCustom, calls=%fused_computation.59 | custom fusion | bytes 32772 | tf_op jit(solution)/shard_map/scatter | solution.py:142
  67.9 6.4 %all-to-all-start.1 = ((f32[16,1,512]{2,1,0:T(1,128)}), f32[16,1,512]{2,1,0:T(1,128)S(1)}, u32[]{:S(2)}, u32[]{:S(2)}) async-start(f32[16,1,512]{2,1,0:T(1,128)} %bitcast.5), calls=%async_computation.1 | async-start | bytes 65536 | tf_op jit(solution)/shard_map/all_to_all | solution.py:150
  74.2 0.0 reduce-scatter.2.cloned.1.call-start
  74.3 0.7 add_select_fusion.1
  75.0 45.9 %all-gather.2.cloned.1.call-done.tok_ref = bf16[4096,8,128]{2,1,0:T(8,128)(2,1)} async-done(((bf16[256,8,128]{2,1,0:T(8,128)(2,1)}), bf16[4096,8,128]{2,1,0:T(8,128)(2,1)}) %all-gather.2.cloned.1.call-update) | async-done | bytes 8388624 | tf_op jit(solution)/shard_map/all_gather | solution.py:128
  120.9 35.3 %request_dots.1 = f32[16,4,128]{2,1,0:T(4,128)} custom-call(s32[8192]{0:T(1024)} %get-tuple-element.5.place_ref, s32[8192]{0:T(1024)} %get-tuple-element.7.row_ref, bf16[4096,8,128]{2,1,0:T(8,128)(2,1)} %all-gather.2.cloned.1.call-done.tok_ref, bf16[4096,8,128]{2,1,0:T(8,128)(2,1)} %bitcast.33), custom_call_target="tpu_custom_call" | custom-call | tf_op jit(solution)/shard_map/request_dots/pallas_call | solution.py:57
  156.2 6.5 %psum.14 = f32[16,4,128]{2,1,0:T(4,128)S(1)} all-reduce(f32[16,4,128]{2,1,0:T(4,128)} %request_dots.1), channel_id=1, replica_groups=mesh['ep'=16,'tp'=2] {'tp'}, use_global_device_ids=true, to_apply=%region_4.5 | all-reduce | flops 8192 | bytes 65536 | tf_op jit(solution)/shard_map/psum | solution.py:154
  162.7 0.6 fusion.15
  163.3 41.3 %mix_rows.1 = bf16[4096,8,128]{2,1,0:T(8,128)(2,1)} custom-call(s32[8192]{0:T(1024)} %get-tuple-element.6.place_ref, s32[8192]{0:T(1024)} %get-tuple-element.7.row_ref, f32[8192]{0:T(1024)} %bitcast.39, bf16[4096,8,128]{2,1,0:T(8,128)(2,1)} %bitcast.32), custom_call_target="tpu_custom_call" | custom-call | tf_op jit(solution)/shard_map/mix_rows/pallas_call | solution.py:106
  204.7 0.0 reduce-scatter.2.cloned.1.call-update
  204.7 179.7 %reduce-scatter.2.cloned.1.call-done = bf16[256,8,128]{2,1,0:T(8,128)(2,1)} async-done(((bf16[4096,8,128]{2,1,0:T(8,128)(2,1)}), bf16[256,8,128]{2,1,0:T(8,128)(2,1)}) %reduce-scatter.2.cloned.1.call-update) | async-done | bytes 524304 | tf_op jit(solution)/shard_map/reduce_scatter | solution.py:157
  384.4 2.1 fusion
  386.4 3.0 psum.15
  389.5 1.4 fusion.2
  390.9 0.9 copy.22
  (12 shorter events, 0.1 us)
Async XLA Ops:
  6.5 114.4 %all-gather.2.cloned.1.call-start = ((), (), s32[]{:S(2)}) async-start(), calls=%async_computation.3 | async-start | bytes 8912896 | tf_op jit(solution)/shard_map/all_gather | solution.py:128
  26.5 41.3 %all-to-all-start = ((s32[16,1,512]{2,1,0:T(1,128)}), s32[16,1,512]{2,1,0:T(1,128)S(1)}, u32[]{:S(2)}, u32[]{:S(2)}) async-start(s32[16,1,512]{2,1,0:T(1,128)} %bitcast.3), calls=%async_computation | async-start | bytes 65536 | tf_op jit(solution)/shard_map/all_to_all | solution.py:144
  67.9 94.8 %all-to-all-start.1 = ((f32[16,1,512]{2,1,0:T(1,128)}), f32[16,1,512]{2,1,0:T(1,128)S(1)}, u32[]{:S(2)}, u32[]{:S(2)}) async-start(f32[16,1,512]{2,1,0:T(1,128)} %bitcast.5), calls=%async_computation.1 | async-start | bytes 65536 | tf_op jit(solution)/shard_map/all_to_all | solution.py:150
  74.2 310.1 %reduce-scatter.2.cloned.1.call-start = ((), (), s32[]{:S(2)}) async-start(), calls=%async_computation.4 | async-start | bytes 8912896 | tf_op jit(solution)/shard_map/reduce_scatter | solution.py:157
  204.7 184.9 %copy-start = (f32[1024]{0:T(1024)S(1)}, f32[1024]{0:T(1024)}, u32[]{:S(2)}) copy-start(f32[1024]{0:T(1024)} %param.11) | copy-start | bytes 12292
Sparse Core Ops, SparseCore 0:
  10.1 110.7 all-gather.1
  204.8 179.5 reduce-scatter.1
